TPU v7x, 128 devices: a whole 4x4x4 slice. The times are simulated.
128 devices in a mesh: sp: 16 (over z, y), dp: 8 (over x, core).
Axes of the slice: x: 4, y: 4, z: 4, core: 2. Of those that a mesh axis runs over, the one named last changes fastest.
Arguments:
- residual: bfloat16 [8, 4096, 2048], P('dp', 'sp'), may hold values from -6 to 6
- queries: bfloat16 [8, 4096, 1024], P('dp', 'sp'), may hold values from -400 to 400
- key_vectors: bfloat16 [8, 4096, 1024], P('dp', 'sp'), may hold values from -6 to 6
- value_vectors: bfloat16 [8, 4096, 1024], P('dp', 'sp'), may hold values from -6 to 6
- gate_cache: float32 [8, 4096, 16], P('dp', 'sp'), may hold values from -514 to 0, as said below
- out_weight: bfloat16 [1024, 2048], P(None, 'dp'), may hold values from -0.1875 to 0.1875
- mix_gain: float32 [2048], replicated, may hold values from 0.1 to 1.9
- route_gain: float32 [2048], replicated, may hold values from 0.1 to 1.9
- out_gain: float32 [2048], replicated, may hold values from 0.1 to 1.9
- routes: int32 [8, 4096, 2], P('dp', 'sp'), may hold values from 0 to 15, all different within a row; in each aligned block of 256 rows (0 to 255, 256 to 511, ..., all dimensions but the last counted through in order) at most 64 rows name the same one
- group_share: float32 [8, 4096], P('dp', 'sp'), may hold values from 0.2 to 1
- expert_share: float32 [8, 4096, 2], P('dp', 'sp'), may hold values from 0.1 to 1
- gate_proj: bfloat16 [16, 2048, 1024], P('sp'), may hold values from -0.125 to 0.125
- up_proj: bfloat16 [16, 2048, 1024], P('sp'), may hold values from -0.125 to 0.125
- down_proj: bfloat16 [16, 1024, 2048], P('sp'), may hold values from -0.1875 to 0.1875
Outputs:
- layer_out: bfloat16 [8, 4096, 2048], P('dp', 'sp')
Inputs may be any that keep to these rules, and one draw needn't show every extreme that they name: `gate_cache`: along the positions of a sequence the values never rise. `routes`: the 2 experts of a position differ. Within the rows of one device (aligned blocks of 256 positions) no expert is named more than 64 times, a bound that some block reaches.
All inputs are finite; a program needn't handle non-finite values.
Results may differ from a plain program's by a relative error of at most 0.0085.
Values may be sent and summed in bfloat16 or wider, within the bound.
No kernel may reach another device: no remote copies, remote signals or barrier semaphores. Data moves between devices by JAX's collectives and lax.ppermute only.
A program may use at most 128 MiB of HBM per device.

v0:
```python
import jax
import jax.numpy as jnp
from jax import lax
from jax.sharding import PartitionSpec as P


def in_one_piece(arrays, axis, split_dim, concat_dim, along):
    ends, at = ([], 0)
    for a in arrays[:-1]:
        at += a.shape[along]
        ends.append(at)
    both = jnp.concatenate(arrays, axis=along)
    return tuple(
        jnp.split(
            lax.all_to_all(both, axis, split_axis=split_dim, concat_axis=concat_dim, tiled=True),
            ends,
            axis=along,
        )
    )


def normalize(values):
    return values * lax.rsqrt(jnp.mean(values * values, axis=-1, keepdims=True) + 1e-06)


def attend(queries, key_rows, value_rows, cum_gates):
    length = queries.shape[0]
    head_count = cum_gates.shape[1]
    head_width = queries.shape[1] // head_count
    score_scale = head_width ** (-0.5)
    q_heads = queries.reshape(length, head_count, head_width)
    k_heads = key_rows.reshape(length, head_count, head_width)
    v_heads = value_rows.reshape(length, head_count, head_width)
    block_rows = min(512, length)
    outputs = []
    for offset in range(0, length, block_rows):
        stop = offset + block_rows
        scores = (
            jnp.einsum(
                "qhd,khd->hqk",
                q_heads[offset:stop],
                k_heads[:stop],
                preferred_element_type=jnp.float32,
            )
            * score_scale
        )
        bias = cum_gates[offset:stop].T[:, :, None] - cum_gates[:stop].T[:, None, :]
        row_pos = offset + jnp.arange(block_rows, dtype=jnp.int32)[:, None]
        col_pos = jnp.arange(stop, dtype=jnp.int32)[None, :]
        scores = jnp.where(col_pos <= row_pos, scores + bias, -1e30)
        row_max = jnp.max(scores, axis=-1, keepdims=True)
        expo_terms = jnp.exp(scores - row_max)
        probs = (expo_terms / jnp.sum(expo_terms, axis=-1, keepdims=True)).astype(jnp.bfloat16)
        mixing = jnp.einsum(
            "hqk,khd->qhd", probs, v_heads[:stop], preferred_element_type=jnp.float32
        )
        outputs.append(mixing.astype(jnp.bfloat16).reshape(block_rows, head_count * head_width))
    return jnp.concatenate(outputs, axis=0)


def body(
    residual,
    queries,
    key_vectors,
    value_vectors,
    gate_cache,
    out_weight,
    mix_gain,
    route_gain,
    out_gain,
    routes,
    group_share,
    expert_share,
    gate_proj,
    up_proj,
    down_proj,
):
    span_size = lax.axis_size("sp")
    tok_rows = residual.shape[1]
    model_width = residual.shape[2]
    by_heads = in_one_piece((queries, key_vectors, value_vectors), "sp", 2, 1, 0)
    cum_gates = lax.all_to_all(gate_cache, "sp", split_axis=2, concat_axis=1, tiled=True)
    attended = attend(by_heads[0][0], by_heads[1][0], by_heads[2][0], cum_gates[0])
    by_tokens = lax.all_to_all(attended[None], "sp", split_axis=1, concat_axis=2, tiled=True)[0]
    mixing = jnp.dot(
        by_tokens,
        lax.all_gather(out_weight, "dp", axis=1, tiled=True),
        preferred_element_type=jnp.float32,
    )
    hidden = (residual[0].astype(jnp.float32) + normalize(mixing) * mix_gain).astype(jnp.bfloat16)
    routed = (normalize(hidden.astype(jnp.float32)) * route_gain).astype(jnp.bfloat16)
    top_count = routes.shape[2]
    experts = span_size * gate_proj.shape[0]
    capacity = 4 * tok_rows // span_size
    assigned = routes[0].reshape(-1)
    expert_ids = jnp.arange(experts, dtype=jnp.int32)
    one_hot = (assigned[:, None] == expert_ids[None, :]).astype(jnp.int32)
    ranking = jnp.sum((jnp.cumsum(one_hot, axis=0) - one_hot) * one_hot, axis=1)
    slot_index = assigned * capacity + ranking
    owners = jnp.arange(assigned.shape[0], dtype=jnp.int32) // top_count
    slot_token = jnp.full((experts * capacity,), tok_rows, jnp.int32).at[slot_index].set(owners)
    padded = jnp.concatenate([routed, jnp.zeros((1, model_width), jnp.bfloat16)], axis=0)
    outgoing = padded[slot_token].reshape(experts, capacity, model_width)
    arrived = lax.all_to_all(outgoing, "sp", split_axis=0, concat_axis=0, tiled=True)
    rows_in = arrived.reshape(-1, model_width)
    gate = jnp.dot(rows_in, gate_proj[0], preferred_element_type=jnp.float32)
    upper = jnp.dot(rows_in, up_proj[0], preferred_element_type=jnp.float32)
    act = (jax.nn.silu(gate) * upper).astype(jnp.bfloat16)
    result = jnp.dot(act, down_proj[0], preferred_element_type=jnp.float32).astype(jnp.bfloat16)
    returned = lax.all_to_all(
        result.reshape(arrived.shape), "sp", split_axis=0, concat_axis=0, tiled=True
    )
    flat_rows = returned.reshape(experts * capacity, model_width)
    gathered = flat_rows[slot_index].reshape(tok_rows, top_count, model_width)
    shares = expert_share[0]
    weights = group_share[0][:, None] * shares / jnp.sum(shares, axis=1, keepdims=True)
    combined = jnp.sum(weights[:, :, None] * gathered.astype(jnp.float32), axis=1)
    layer_out = (hidden.astype(jnp.float32) + combined * out_gain).astype(jnp.bfloat16)
    return layer_out[None]


def solution(mesh):
    placed = (
        P("dp", "sp", None),
        P("dp", "sp", None),
        P("dp", "sp", None),
        P("dp", "sp", None),
        P("dp", "sp", None),
        P(None, "dp"),
        P(),
        P(),
        P(),
        P("dp", "sp", None),
        P("dp", "sp"),
        P("dp", "sp", None),
        P("sp", None, None),
        P("sp", None, None),
        P("sp", None, None),
    )
    return jax.shard_map(
        body, mesh=mesh, in_specs=placed, out_specs=P("dp", "sp", None), check_vma=False
    )
```

profile of v0, /device:TPU:0, one launch (start us, length us, event | category | flops | bytes accessed | tf_op | source)
XLA Modules:
  0.0 329.0 jit_solution(18312201517383455463)
XLA Ops:
  7.9 8.2 %all-to-all-start.1 = ((f32[1,256,16]{1,0,2:T(1,128)}), f32[1,256,16]{1,0,2:T(1,128)S(1)}, u32[]{:S(2)}, u32[]{:S(2)}) async-start(f32[1,256,16]{1,0,2:T(1,128)} %copy.92), calls=%async_computation.1 | async-start | bytes 32768 | tf_op jit(solution)/shard_map/all_to_all | solution.py:82
  16.8 2.4 copy.85
  25.7 4.6 %pad_maximum_fusion = bf16[3,256,1024]{1,0,2:T(4,128)(2,1)} fusion(bf16[1,256,1024]{1,0,2:T(2,128)(2,1)S(1)} %copy.87, bf16[1,256,1024]{1,0,2:T(2,128)(2,1)S(1)} %copy.86, bf16[1,256,1024]{1,0,2:T(2,128)(2,1)S(1)} %copy.85), kind=kLoop, calls=%fused_computation.55 | loop fusion | flops 4718592 | bytes 3145728 | tf_op jit(solution)/shard_map/concatenate | solution.py:12
  30.3 7.7 %all-to-all-start = ((bf16[3,256,1024]{1,0,2:T(4,128)(2,1)}), bf16[3,256,1024]{1,0,2:T(4,128)(2,1)S(1)}, u32[]{:S(2)}, u32[]{:S(2)}) async-start(bf16[3,256,1024]{1,0,2:T(4,128)(2,1)} %pad_maximum_fusion), calls=%async_computation | async-start | bytes 4194304 | tf_op jit(solution)/shard_map/all_to_all | solution.py:15
  38.6 29.3 %all-to-all-done = bf16[3,256,1024]{1,0,2:T(4,128)(2,1)S(1)} async-done(((bf16[3,256,1024]{1,0,2:T(4,128)(2,1)}), bf16[3,256,1024]{1,0,2:T(4,128)(2,1)S(1)}, u32[]{:S(2)}, u32[]{:S(2)}) %all-to-all-start) | async-done | bytes 1572896 | tf_op jit(solution)/shard_map/all_to_all | solution.py:15
  90.9 2.4 fusion.85
  94.7 2.6 fusion.50
  105.1 2.8 fusion.40
  107.9 4.9 %copy.114 = bf16[1,4096,64]{2,0,1:T(2,128)(2,1)S(1)} copy(bf16[1,4096,64]{1,2,0:T(8,128)(2,1)} %bitcast.333) | data formatting | bytes 1048576 | tf_op jit(solution)/shard_map/broadcast_in_dim | solution.py:84
  113.3 22.4 %reduce.41 = bf16[4096,64]{1,0:T(8,128)(2,1)S(1)} reduce(bf16[4096,1,64]{2,1,0:T(2,128)(2,1)S(1)} %bitcast.315, bf16[]{:T(256)} %broadcast.266), dimensions={1}, to_apply=%bitcast.272.reduce_sub_computation | reduce | bytes 1048578
  137.2 3.6 %all-to-all-start.2 = ((bf16[16,2,8192]{2,1,0:T(2,128)(2,1)}), bf16[16,2,8192]{2,1,0:T(2,128)(2,1)S(1)}, u32[]{:S(2)}, u32[]{:S(2)}) async-start(bf16[16,2,8192]{2,1,0:T(2,128)(2,1)} %reshape.637), calls=%async_computation.2 | async-start | bytes 1048576 | tf_op jit(solution)/shard_map/all_to_all | solution.py:84
  141.1 2.4 scatter_custom_fusion
  143.6 8.5 %all-to-all-done.2 = bf16[16,2,8192]{2,1,0:T(2,128)(2,1)S(1)} async-done(((bf16[16,2,8192]{2,1,0:T(2,128)(2,1)}), bf16[16,2,8192]{2,1,0:T(2,128)(2,1)S(1)}, u32[]{:S(2)}, u32[]{:S(2)}) %all-to-all-start.2) | async-done | bytes 524320 | tf_op jit(solution)/shard_map/all_to_all | solution.py:84
  156.0 3.7 %multiply_reduce_fusion.1 = (f32[256]{0:T(256)S(1)}, f32[256,2048]{1,0:T(8,128)S(1)}) fusion(bf16[256,1024]{0,1:T(8,128)(2,1)S(1)} %bitcast.336, bf16[1024,2048]{1,0:T(8,128)(2,1)} %all-gather.2.cloned.1.call-done), kind=kOutput, calls=%fused_computation.58 | convolution fusion | flops 1074790144 | bytes 6816768 | tf_op jit(solution)/shard_map/dot_general | solution.py:85
  160.7 6.0 %gather_fusion = bf16[1024,2048]{1,0:T(8,128)(2,1)} fusion(bf16[257,2048]{1,0:T(8,128)(2,1)S(1)} %concatenate.11, s32[1024]{0:T(1024)S(1)} %fusion.61), kind=kCustom, calls=%fused_computation | custom fusion | bytes 8392704 | tf_op jit(solution)/shard_map/gather | solution.py:103
  166.7 54.6 %all_to_all.55 = bf16[16,64,2048]{2,1,0:T(8,128)(2,1)S(1)} all-to-all(bf16[16,64,2048]{2,1,0:T(8,128)(2,1)} %bitcast.313), channel_id=1, replica_groups=mesh['sp'=16,'dp'=8] {'sp'}, dimensions={0} | all-to-all | bytes 8388608 | tf_op jit(solution)/shard_map/all_to_all | solution.py:104
  221.3 4.5 %fusion.6 = f32[1024,1024]{1,0:T(8,128)S(1)} fusion(bf16[1024,2048]{1,0:T(8,128)(2,1)S(1)} %bitcast.317, bf16[1,2048,1024]{2,1,0:T(8,128)(2,1)S(1)} %copy-done.14), kind=kOutput, calls=%fused_computation.25 | convolution fusion | flops 4294967296 | bytes 12582912 | tf_op jit(solution)/shard_map/dot_general | solution.py:107
  225.9 5.4 %multiply_convert_fusion = bf16[1024,1024]{1,0:T(8,128)(2,1)S(1)} fusion(f32[1024,1024]{1,0:T(8,128)S(1)} %fusion.6, bf16[1024,2048]{1,0:T(8,128)(2,1)S(1)} %bitcast.318, bf16[1,2048,1024]{2,1,0:T(8,128)(2,1)S(1)} %copy-done.15), kind=kOutput, calls=%fused_computation.30 | convolution fusion | flops 4301258752 | bytes 14680064 | tf_op jit(solution)/shard_map/dot_general | solution.py:106
  231.3 6.1 %fusion.11 = bf16[1024,2048]{1,0:T(8,128)(2,1)} fusion(bf16[1024,1024]{1,0:T(8,128)(2,1)S(1)} %multiply_convert_fusion, bf16[1,1024,2048]{2,1,0:T(8,128)(2,1)S(1)} %copy-done.16), kind=kOutput, calls=%fused_computation.36 | convolution fusion | flops 4297064448 | bytes 10485760 | tf_op jit(solution)/shard_map/dot_general | solution.py:109
  237.4 4.8 %all-to-all-start.4 = ((bf16[16,64,2048]{2,1,0:T(8,128)(2,1)}), bf16[16,64,2048]{2,1,0:T(8,128)(2,1)}, u32[]{:S(2)}, u32[]{:S(2)}) async-start(bf16[16,64,2048]{2,1,0:T(8,128)(2,1)} %bitcast.316), calls=%async_computation.4 | async-start | bytes 8388608 | tf_op jit(solution)/shard_map/all_to_all | solution.py:110
  242.5 58.1 %all-to-all-done.4 = bf16[16,64,2048]{2,1,0:T(8,128)(2,1)} async-done(((bf16[16,64,2048]{2,1,0:T(8,128)(2,1)}), bf16[16,64,2048]{2,1,0:T(8,128)(2,1)}, u32[]{:S(2)}, u32[]{:S(2)}) %all-to-all-start.4) | async-done | bytes 4194336 | tf_op jit(solution)/shard_map/all_to_all | solution.py:110
  300.6 7.1 %gather_fusion.1 = bf16[512,2048]{1,0:T(8,128)(2,1)S(1)} fusion(bf16[1024,2048]{1,0:T(8,128)(2,1)} %bitcast.57, s32[1024]{0:T(1024)S(1)} %pad_clamp_fusion), kind=kCustom, calls=%fused_computation.1 | custom fusion | bytes 4196352 | tf_op jit(solution)/shard_map/gather | solution.py:114
  307.7 4.0 %reshape.605 = f32[256,2,2048]{2,1,0:T(2,128)} reshape(bf16[512,2048]{1,0:T(8,128)(2,1)S(1)} %gather_fusion.1) | data formatting | bytes 6291456 | tf_op jit(solution)/shard_map/convert_element_type | solution.py:117
  311.7 8.9 %multiply_reduce_fusion = f32[256,2048]{1,0:T(8,128)S(1)} fusion(f32[256,2,2048]{2,1,0:T(2,128)} %reshape.605, f32[256,2]{1,0:T(8,128)S(1)} %copy.117), kind=kLoop, calls=%fused_computation.29 | loop fusion | flops 1572864 | bytes 6293504 | tf_op jit(solution)/shard_map/reduce_sum | solution.py:117
  (155 shorter events, 49.5 us)
Async XLA Ops:
  6.5 17.5 %copy-start.11 = (s32[1,256,2]{1,2,0:T(2,128)S(1)}, s32[1,256,2]{1,2,0:T(2,128)}, u32[]{:S(2)}) copy-start(s32[1,256,2]{1,2,0:T(2,128)} %param.24) | copy-start | bytes 6148
  7.9 22.4 %all-to-all-start.1 = ((f32[1,256,16]{1,0,2:T(1,128)}), f32[1,256,16]{1,0,2:T(1,128)S(1)}, u32[]{:S(2)}, u32[]{:S(2)}) async-start(f32[1,256,16]{1,0,2:T(1,128)} %copy.92), calls=%async_computation.1 | async-start | bytes 32768 | tf_op jit(solution)/shard_map/all_to_all | solution.py:82
  16.1 139.9 %all-gather.2.cloned.1.call-start = ((), (), s32[]{:S(2)}) async-start(), calls=%async_computation.5 | async-start | bytes 4718592 | tf_op jit(solution)/shard_map/all_gather | solution.py:87
  30.3 37.6 %all-to-all-start = ((bf16[3,256,1024]{1,0,2:T(4,128)(2,1)}), bf16[3,256,1024]{1,0,2:T(4,128)(2,1)S(1)}, u32[]{:S(2)}, u32[]{:S(2)}) async-start(bf16[3,256,1024]{1,0,2:T(4,128)(2,1)} %pad_maximum_fusion), calls=%async_computation | async-start | bytes 4194304 | tf_op jit(solution)/shard_map/all_to_all | solution.py:15
  81.4 7.7 %copy-start = (f32[512,2048]{1,0:T(8,128)}, f32[512,2048]{1,0:T(8,128)S(1)}, u32[]{:S(2)}) copy-start(f32[512,2048]{1,0:T(8,128)S(1)} %get-tuple-element.46) | copy-start | bytes 12582916
  94.6 2.6 copy-start.1
  94.6 2.6 copy-start.7
  97.2 1.7 copy-start.6
  98.9 1.9 copy-start.5
  100.8 2.1 copy-start.4
  102.8 2.3 copy-start.3
  137.2 14.9 %all-to-all-start.2 = ((bf16[16,2,8192]{2,1,0:T(2,128)(2,1)}), bf16[16,2,8192]{2,1,0:T(2,128)(2,1)S(1)}, u32[]{:S(2)}, u32[]{:S(2)}) async-start(bf16[16,2,8192]{2,1,0:T(2,128)(2,1)} %reshape.637), calls=%async_computation.2 | async-start | bytes 1048576 | tf_op jit(solution)/shard_map/all_to_all | solution.py:84
  155.8 3.9 %copy-start.2 = (bf16[1,256,2048]{2,1,0:T(8,128)(2,1)S(1)}, bf16[1,256,2048]{2,1,0:T(8,128)(2,1)}, u32[]{:S(2)}) copy-start(bf16[1,256,2048]{2,1,0:T(8,128)(2,1)} %param.15) | copy-start | bytes 3145732
  155.8 3.9 %copy-start.8 = (f32[2048]{0:T(1024)S(1)}, f32[2048]{0:T(1024)}, u32[]{:S(2)}) copy-start(f32[2048]{0:T(1024)} %param.21) | copy-start | bytes 24580
  156.0 4.3 %copy-start.9 = (f32[2048]{0:T(1024)S(1)}, f32[2048]{0:T(1024)}, u32[]{:S(2)}) copy-start(f32[2048]{0:T(1024)} %param.22) | copy-start | bytes 24580
  166.7 54.6 %copy-start.14 = (bf16[1,2048,1024]{2,1,0:T(8,128)(2,1)S(1)}, bf16[1,2048,1024]{2,1,0:T(8,128)(2,1)}, u32[]{:S(2)}) copy-start(bf16[1,2048,1024]{2,1,0:T(8,128)(2,1)} %param.28) | copy-start | bytes 12582916
  221.3 4.5 %copy-start.15 = (bf16[1,2048,1024]{2,1,0:T(8,128)(2,1)S(1)}, bf16[1,2048,1024]{2,1,0:T(8,128)(2,1)}, u32[]{:S(2)}) copy-start(bf16[1,2048,1024]{2,1,0:T(8,128)(2,1)} %param.27) | copy-start | bytes 12582916
  225.9 5.4 %copy-start.16 = (bf16[1,1024,2048]{2,1,0:T(8,128)(2,1)S(1)}, bf16[1,1024,2048]{2,1,0:T(8,128)(2,1)}, u32[]{:S(2)}) copy-start(bf16[1,1024,2048]{2,1,0:T(8,128)(2,1)} %param.29) | copy-start | bytes 12582916
  237.4 4.9 %copy-start.12 = (f32[1,256,2]{1,2,0:T(2,128)S(1)}, f32[1,256,2]{1,2,0:T(2,128)}, u32[]{:S(2)}) copy-start(f32[1,256,2]{1,2,0:T(2,128)} %param.26) | copy-start | bytes 6148
  237.4 4.9 %copy-start.13 = (f32[1,256]{1,0:T(1,128)S(1)}, f32[1,256]{1,0:T(1,128)}, u32[]{:S(2)}) copy-start(f32[1,256]{1,0:T(1,128)} %param.25) | copy-start | bytes 3076
  237.4 63.2 %all-to-all-start.4 = ((bf16[16,64,2048]{2,1,0:T(8,128)(2,1)}), bf16[16,64,2048]{2,1,0:T(8,128)(2,1)}, u32[]{:S(2)}, u32[]{:S(2)}) async-start(bf16[16,64,2048]{2,1,0:T(8,128)(2,1)} %bitcast.316), calls=%async_computation.4 | async-start | bytes 8388608 | tf_op jit(solution)/shard_map/all_to_all | solution.py:110
  311.7 8.9 %copy-start.10 = (f32[2048]{0:T(1024)S(1)}, f32[2048]{0:T(1024)}, u32[]{:S(2)}) copy-start(f32[2048]{0:T(1024)} %param.23) | copy-start | bytes 24580
Sparse Core Ops, SparseCore 0:
  18.5 37.0 all-gather.1
where the time goes:
time: 333 us; the launch traced here: 329 us
  waiting for transfers between devices  96.7 us (29%)
  blocking collectives  54.6 us (16%)
  matrix products  46.7 us (14%)
  local copies, waits for them, and re-layouts  46.6 us (14%)
  other arithmetic  45.8 us (14%)
  starting transfers between devices  24.4 us (7%)
  between operations  14.4 us (4%)
    all_to_all x1, waiting for transfers between devices, body(): lax.all_to_all(result.reshape(arrived.shape), 'sp', split_axis=0, concat_...  58.1 us
    all_to_all x1, blocking collectives, body(): lax.all_to_all(outgoing, 'sp', split_axis=0, concat_axis=0, tiled=True)  54.6 us
    all_to_all x1, waiting for transfers between devices, in_one_piece(): lax.all_to_all(both, axis, split_axis=split_dim, concat_axis=concat_dim,...  29.3 us
    unnamed x1, other arithmetic  22.4 us
    unnamed x67, local copies, waits for them, and re-layouts  17.1 us
    dot_general x8, matrix products, attend(): jnp.einsum('hqk,khd->qhd', probs, v_heads[:stop], preferred_element_type=...  15.4 us
    dot_general x8, matrix products, attend(): jnp.einsum('qhd,khd->hqk', q_heads[offset:stop], k_heads[:stop], preferre...  11.6 us
    reduce_sum x1, other arithmetic, body(): jnp.sum(weights[:, :, None] * gathered.astype(jnp.float32), axis=1)  8.89 us
  transfers between devices with their start and end apart: 5, of which 3 were waited for; matrix products, arithmetic and copies ran while one was open for 27% of the time, Pallas kernels for 0%

commit v1 on v0

v1 whole, which is shorter than its diff:
```python
import jax
import jax.numpy as jnp
from jax import lax
from jax.experimental import pallas as pl
from jax.experimental.pallas import tpu as pltpu
from jax.sharding import PartitionSpec as P

F32 = jnp.float32
BF16 = jnp.bfloat16
HD = 64
SLOTS = 64
NEG = -1e30


def vmem(mib):
    return pltpu.CompilerParams(vmem_limit_bytes=mib * 1024 * 1024)


def vspec():
    return pl.BlockSpec(memory_space=pltpu.VMEM)


def pack_kernel(q_ref, k_ref, v_ref, g_ref, o_ref):
    rows = q_ref.shape[0]
    half = rows // 2
    heads = g_ref.shape[1]
    gates = jnp.concatenate([g_ref[...], jnp.zeros((rows, 128 - heads), F32)], axis=1).T
    hi = gates.astype(BF16).astype(F32)
    mid = (gates - hi).astype(BF16).astype(F32)
    low = gates - hi - mid
    for pair in range(heads // 2):
        cols = slice(128 * pair, 128 * pair + 128)
        q, k, v = q_ref[:, cols], k_ref[:, cols], v_ref[:, cols]
        for side in range(2):
            h = 2 * pair + side
            at = slice(64 * side, 64 * side + 64)
            o_ref[h, 0:rows, :] = jnp.concatenate([q[:, at], k[:, at]], axis=1)
            o_ref[h, rows:rows + half, :] = jnp.concatenate([v[:half, at], v[half:, at]], axis=1)
            terms = [t[h:h + 1, 128 * j:128 * j + 128] for t in (hi, mid, low) for j in range(2)]
            terms.append(jnp.zeros((10, 128), F32))
            o_ref[h, rows + half:rows + half + 16, :] = jnp.concatenate(terms, axis=0).astype(BF16)


def pack(q, k, v, g):
    rows, heads = q.shape[0], g.shape[1]
    return pl.pallas_call(
        pack_kernel,
        out_shape=jax.ShapeDtypeStruct((heads, rows + rows // 2 + 16, 128), BF16),
        in_specs=[vspec()] * 4,
        out_specs=vspec(),
        compiler_params=vmem(40),
        name="pack",
    )(q, k, v, g)


def attend_kernel(x_ref, o_ref, q_scr, k_scr, v_scr, g_scr, s_scr):
    blocks = x_ref.shape[0]
    rows = (x_ref.shape[1] - 16) * 2 // 3
    half = rows // 2
    lane = lax.broadcasted_iota(jnp.int32, (128, 64), 1)
    lane2 = lax.broadcasted_iota(jnp.int32, (rows, 64), 1)
    minus = jnp.where(lane2 < 3, -1.0, 0.0).astype(BF16)
    ones = jnp.where(lane2 < 1, 1.0, 0.0).astype(BF16)
    g_scr[...] = jnp.zeros_like(g_scr)
    for b in range(blocks):
        t = x_ref[b, rows + half:rows + half + 16, :].astype(F32)
        g_scr[2 * b:2 * b + 2, :] = t[0:2] + t[2:4] + t[4:6]
    gates = g_scr[...].T
    for b in range(blocks):
        base = b * rows
        qk = x_ref[b, 0:rows, :]
        q = (qk[:, 0:64].astype(F32) * (HD ** -0.5)).astype(BF16)
        q_scr[base:base + rows, :] = jnp.concatenate([q, minus], axis=1)
        for j in range(2):
            c = gates[:, 2 * b + j:2 * b + j + 1]
            hi = c.astype(BF16).astype(F32)
            mid = (c - hi).astype(BF16).astype(F32)
            low = c - hi - mid
            ext = jnp.where(lane == 0, hi, jnp.where(lane == 1, mid, jnp.where(lane == 2, low, 0.0)))
            k_scr[base + 128 * j:base + 128 * j + 128, :] = jnp.concatenate(
                [qk[128 * j:128 * j + 128, 64:128], ext.astype(BF16)], axis=1)
        vv = x_ref[b, rows:rows + half, :]
        v_scr[base:base + half, :] = jnp.concatenate([vv[:, 0:64], ones[:half]], axis=1)
        v_scr[base + half:base + rows, :] = jnp.concatenate([vv[:, 64:128], ones[:half]], axis=1)

    tile = 2 * rows
    nt = (((1,), (1,)), ((), ()))

    def top_of(s):
        m = s[:, 0:128]
        for j in range(1, tile // 128):
            m = jnp.maximum(m, s[:, 128 * j:128 * j + 128])
        return m

    def q_tile(qi, _):
        q = q_scr[pl.ds(qi * tile, tile), :]

        def scores(kj, m):
            s = lax.dot_general(q, k_scr[pl.ds(kj * tile, tile), :], nt, preferred_element_type=F32)
            s_scr[kj] = s
            return jnp.maximum(m, top_of(s))

        m = lax.fori_loop(0, qi, scores, jnp.full((tile, 128), NEG, F32))
        s = lax.dot_general(q, k_scr[pl.ds(qi * tile, tile), :], nt, preferred_element_type=F32)
        r = lax.broadcasted_iota(jnp.int32, (tile, tile), 0)
        c = lax.broadcasted_iota(jnp.int32, (tile, tile), 1)
        s = jnp.where(c <= r, s, NEG)
        m = jnp.max(jnp.maximum(m, top_of(s)), axis=1, keepdims=True)
        p = jnp.exp(s - m).astype(BF16)
        acc = jnp.dot(p, v_scr[pl.ds(qi * tile, tile), :], preferred_element_type=F32)

        def mixing(kj, acc):
            p = jnp.exp(s_scr[kj] - m).astype(BF16)
            return acc + jnp.dot(p, v_scr[pl.ds(kj * tile, tile), :], preferred_element_type=F32)

        acc = lax.fori_loop(0, qi, mixing, acc)
        out = acc[:, 0:64] / acc[:, 64:65]
        for j in range(2):
            top = out[j * rows:j * rows + half]
            bottom = out[j * rows + half:(j + 1) * rows]
            o_ref[2 * qi + j] = jnp.concatenate([top, bottom], axis=1).astype(BF16)
        return 0

    lax.fori_loop(0, blocks // 2, q_tile, 0)


def attend(x):
    blocks = x.shape[0]
    rows = (x.shape[1] - 16) * 2 // 3
    length = blocks * rows
    return pl.pallas_call(
        attend_kernel,
        out_shape=jax.ShapeDtypeStruct((blocks, rows // 2, 128), BF16),
        in_specs=[vspec()],
        out_specs=vspec(),
        scratch_shapes=[
            pltpu.VMEM((length, 128), BF16),
            pltpu.VMEM((length, 128), BF16),
            pltpu.VMEM((length, 128), BF16),
            pltpu.VMEM((128, 128), F32),
            pltpu.VMEM((blocks // 2, 2 * rows, 2 * rows), F32),
        ],
        compiler_params=vmem(48),
        name="attend",
    )(x)


def route_kernel(r_ref, gs_ref, es_ref, pa_ref, pb_ref, ca_ref, cb_ref):
    rows = r_ref.shape[0]
    experts = pa_ref.shape[0] // (SLOTS // 2)
    half = SLOTS // 2
    e0, e1 = r_ref[:, 0:1], r_ref[:, 1:2]
    lane = lax.broadcasted_iota(jnp.int32, (rows, 128), 1)
    named = jnp.where((lane == e0) | (lane == e1), 1.0, 0.0)
    ri = lax.broadcasted_iota(jnp.int32, (rows, rows), 0)
    ci = lax.broadcasted_iota(jnp.int32, (rows, rows), 1)
    before = jnp.where(ci < ri, 1.0, 0.0).astype(BF16)
    rank = jnp.dot(before, named.astype(BF16), preferred_element_type=F32)
    place = jnp.where(named > 0, rank, -1.0)
    by_expert = place.T
    slot_row = lax.broadcasted_iota(jnp.int32, (half, rows), 0).astype(F32)
    for e in range(experts):
        mine = by_expert[e:e + 1, :]
        pa_ref[e * half:(e + 1) * half, :] = jnp.where(mine == slot_row, 1.0, 0.0).astype(BF16)
        pb_ref[e * half:(e + 1) * half, :] = jnp.where(mine == slot_row + half, 1.0, 0.0).astype(BF16)
    share = jnp.sum(jnp.where(ri == ci, gs_ref[...], 0.0), axis=1, keepdims=True)
    s0, s1 = es_ref[:, 0:1], es_ref[:, 1:2]
    total = s0 + s1
    w0, w1 = share * s0 / total, share * s1 / total
    k0 = jnp.sum(jnp.where(lane == e0, rank, 0.0), axis=1, keepdims=True).astype(jnp.int32)
    k1 = jnp.sum(jnp.where(lane == e1, rank, 0.0), axis=1, keepdims=True).astype(jnp.int32)
    at = lax.broadcasted_iota(jnp.int32, (rows, experts * half), 1)
    for ref, low in ((ca_ref, 0), (cb_ref, half)):
        a0 = jnp.where((k0 >= low) & (k0 < low + half), e0 * half + k0 - low, -1)
        a1 = jnp.where((k1 >= low) & (k1 < low + half), e1 * half + k1 - low, -1)
        w = jnp.where(at == a0, w0, jnp.where(at == a1, w1, 0.0))
        hi = w.astype(BF16)
        ref[0:rows, :] = hi
        ref[rows:2 * rows, :] = (w - hi.astype(F32)).astype(BF16)


def route_tables(routes, group_share, expert_share, experts):
    rows = routes.shape[0]
    n = experts * SLOTS // 2
    p_shape = jax.ShapeDtypeStruct((n, rows), BF16)
    c_shape = jax.ShapeDtypeStruct((2 * rows, n), BF16)
    return pl.pallas_call(
        route_kernel,
        out_shape=(p_shape, p_shape, c_shape, c_shape),
        in_specs=[vspec()] * 3,
        out_specs=(vspec(),) * 4,
        compiler_params=vmem(32),
        name="route_tables",
    )(routes, group_share, expert_share)


def project_kernel(a_ref, w_ref, res_ref, mg_ref, rg_ref, p_ref, hid_ref, routed_ref, out_ref):
    heads, half = a_ref.shape[0], a_ref.shape[1]
    left = lax.broadcasted_iota(jnp.int32, (half, 128), 1) < 64
    tops, bottoms = [], []
    for pair in range(heads // 2):
        a = a_ref[2 * pair]
        b = a_ref[2 * pair + 1]
        tops.append(jnp.concatenate([a[:, 0:64], b[:, 0:64]], axis=1))
        bottoms.append(jnp.concatenate([a[:, 64:128], b[:, 64:128]], axis=1))
    att = jnp.concatenate([jnp.concatenate(tops, axis=1), jnp.concatenate(bottoms, axis=1)], axis=0)
    mixed = jnp.dot(att, w_ref[...], preferred_element_type=F32)
    scale = lax.rsqrt(jnp.mean(mixed * mixed, axis=1, keepdims=True) + 1e-6)
    hidden = (res_ref[...].astype(F32) + mixed * scale * mg_ref[...]).astype(BF16)
    hid_ref[...] = hidden
    h = hidden.astype(F32)
    routed = (h * lax.rsqrt(jnp.mean(h * h, axis=1, keepdims=True) + 1e-6) * rg_ref[...]).astype(BF16)
    routed_ref[...] = routed
    out_ref[...] = jnp.dot(p_ref[...], routed, preferred_element_type=F32).astype(BF16)


def project(att, weight, residual, mix_gain, route_gain, table):
    rows, width = residual.shape
    flat = jax.ShapeDtypeStruct((rows, width), BF16)
    return pl.pallas_call(
        project_kernel,
        out_shape=(flat, flat, jax.ShapeDtypeStruct((table.shape[0], width), BF16)),
        in_specs=[vspec()] * 6,
        out_specs=(vspec(),) * 3,
        compiler_params=vmem(48),
        name="project",
    )(att, weight, residual, mix_gain, route_gain, table)


def select_kernel(p_ref, x_ref, o_ref):
    o_ref[...] = jnp.dot(p_ref[...], x_ref[...], preferred_element_type=F32).astype(BF16)


def select_rows(table, x):
    return pl.pallas_call(
        select_kernel,
        out_shape=jax.ShapeDtypeStruct((table.shape[0], x.shape[1]), BF16),
        in_specs=[vspec()] * 2,
        out_specs=vspec(),
        compiler_params=vmem(32),
        name="select_rows",
    )(table, x)


def expert_kernel(x_ref, g_ref, u_ref, d_ref, o_ref, act_scr, acc_scr):
    f = pl.program_id(0)
    x = x_ref[...]
    gate = jnp.dot(x, g_ref[...], preferred_element_type=F32)
    upper = jnp.dot(x, u_ref[...], preferred_element_type=F32)
    act = (gate / (1.0 + jnp.exp(-gate)) * upper).astype(BF16)
    part = jnp.dot(act, d_ref[...], preferred_element_type=F32)

    @pl.when(f == 0)
    def _():
        acc_scr[...] = part

    @pl.when((f > 0) & (f < pl.num_programs(0) - 1))
    def _():
        acc_scr[...] += part

    @pl.when(f == pl.num_programs(0) - 1)
    def _():
        o_ref[...] = (acc_scr[...] + part).astype(BF16)


def expert(x, gate, up, down, tile=512):
    rows, width = x.shape
    ff = gate.shape[1]
    return pl.pallas_call(
        expert_kernel,
        grid=(ff // tile,),
        out_shape=jax.ShapeDtypeStruct((rows, width), BF16),
        in_specs=[
            pl.BlockSpec((rows, width), lambda f: (0, 0)),
            pl.BlockSpec((width, tile), lambda f: (0, f)),
            pl.BlockSpec((width, tile), lambda f: (0, f)),
            pl.BlockSpec((tile, width), lambda f: (f, 0)),
        ],
        out_specs=pl.BlockSpec((rows, width), lambda f: (0, 0)),
        scratch_shapes=[pltpu.VMEM((8, 128), BF16), pltpu.VMEM((rows, width), F32)],
        compiler_params=vmem(56),
        cost_estimate=pl.CostEstimate(flops=6 * rows * width * ff, transcendentals=rows * ff, bytes_accessed=16000000),
        name="expert",
    )(x, gate, up, down)


def gather_kernel(c_ref, x_ref, o_ref):
    rows = o_ref.shape[0]
    both = jnp.dot(c_ref[...], x_ref[...], preferred_element_type=F32)
    o_ref[...] = both[:rows] + both[rows:]


def gather_sum(table, x):
    return pl.pallas_call(
        gather_kernel,
        out_shape=jax.ShapeDtypeStruct((table.shape[0] // 2, x.shape[1]), F32),
        in_specs=[vspec()] * 2,
        out_specs=vspec(),
        compiler_params=vmem(32),
        name="gather_sum",
    )(table, x)


def finish_kernel(c_ref, x_ref, first_ref, hid_ref, og_ref, o_ref):
    rows = o_ref.shape[0]
    both = jnp.dot(c_ref[...], x_ref[...], preferred_element_type=F32)
    combined = first_ref[...] + both[:rows] + both[rows:]
    o_ref[...] = (hid_ref[...].astype(F32) + combined * og_ref[...]).astype(BF16)


def finish(table, x, first, hidden, out_gain):
    return pl.pallas_call(
        finish_kernel,
        out_shape=jax.ShapeDtypeStruct(hidden.shape, BF16),
        in_specs=[vspec()] * 5,
        out_specs=vspec(),
        compiler_params=vmem(40),
        name="finish",
    )(table, x, first, hidden, out_gain)


def swap(x):
    return lax.all_to_all(x, "sp", split_axis=0, concat_axis=0, tiled=True)


def body(
    residual,
    queries,
    key_vectors,
    value_vectors,
    gate_cache,
    out_weight,
    mix_gain,
    route_gain,
    out_gain,
    routes,
    group_share,
    expert_share,
    gate_proj,
    up_proj,
    down_proj,
):
    experts = lax.axis_size("sp")
    width = residual.shape[2]
    weight = lax.all_gather(out_weight, "dp", axis=1, tiled=True)
    arrived = swap(pack(queries[0], key_vectors[0], value_vectors[0], gate_cache[0]))
    pa, pb, ca, cb = route_tables(routes[0], group_share, expert_share[0], experts)
    att = swap(attend(arrived))
    hidden, routed, rows_a = project(
        att, weight, residual[0], mix_gain[None], route_gain[None], pa)

    def exchange(x):
        return swap(x.reshape(experts, SLOTS // 2, width)).reshape(x.shape)

    in_a = exchange(rows_a)
    in_b = exchange(select_rows(pb, routed))
    out_a = exchange(expert(in_a, gate_proj[0], up_proj[0], down_proj[0]))
    out_b = exchange(expert(in_b, gate_proj[0], up_proj[0], down_proj[0]))
    first = gather_sum(ca, out_a)
    return finish(cb, out_b, first, hidden, out_gain[None])[None]


def solution(mesh):
    placed = (
        P("dp", "sp", None),
        P("dp", "sp", None),
        P("dp", "sp", None),
        P("dp", "sp", None),
        P("dp", "sp", None),
        P(None, "dp"),
        P(),
        P(),
        P(),
        P("dp", "sp", None),
        P("dp", "sp"),
        P("dp", "sp", None),
        P("sp", None, None),
        P("sp", None, None),
        P("sp", None, None),
    )
    return jax.shard_map(
        body, mesh=mesh, in_specs=placed, out_specs=P("dp", "sp", None), check_vma=False
    )
```

time: 333 us -> 246 us (0.74)
  Pallas kernels: 0 us -> 70.8 us
  matrix products: 46.7 us -> 0 us
  other arithmetic: 45.8 us -> 0 us
  local copies, waits for them, and re-layouts: 46.6 us -> 13.3 us
  blocking collectives: 54.6 us -> 31.5 us
  starting transfers between devices: 24.4 us -> 20.1 us
    pallas_call x0 -> x9, Pallas kernels: none -> 70.8 us  [the longest x1 29.8 us: attend(): pl.pallas_call(attend_kernel, out_shape=jax.ShapeDtypeStruct((blocks, row...]
    dot_general x20 -> x0, matrix products: 46.7 us -> none  [the longest x8 15.4 us: attend(): jnp.einsum('hqk,khd->qhd', probs, v_heads[:stop], preferred_element_type=...]
    all_to_all x1, blocking collectives: 54.6 us -> 31.5 us  [swap(): return lax.all_to_all(x, 'sp', split_axis=0, concat_axis=0, tiled=True)]
    unnamed x1 -> x0, other arithmetic: 22.4 us -> none
    reduce_sum x12 -> x0, other arithmetic: 15.9 us -> none  [the longest x1 8.89 us: body(): jnp.sum(weights[:, :, None] * gathered.astype(jnp.float32), axis=1)]
    gather x2 -> x0, local copies, waits for them, and re-layouts: 13.2 us -> none  [the longest x1 7.13 us: body(): gathered = flat_rows[slot_index].reshape(tok_rows, top_count, model_width)]
    broadcast_in_dim x1 -> x0, local copies, waits for them, and re-layouts: 4.86 us -> none  [body(): attended[None]]
    concatenate x1 -> x0, other arithmetic: 4.56 us -> none  [in_one_piece(): both = jnp.concatenate(arrays, axis=along)]
  transfers between devices with their start and end apart: 5 -> 6, of which waited for: 3 -> 5; matrix products, arithmetic and copies ran while one was open for 27% -> 0% of each run, Pallas kernels for 0% -> 25%
where the time goes in v1:
time: 246 us; the launch traced here: 245 us
  waiting for transfers between devices  95.5 us (39%)
  Pallas kernels  70.8 us (29%)
  blocking collectives  31.5 us (13%)
  starting transfers between devices  20.1 us (8%)
  between operations  13.6 us (6%)
  local copies, waits for them, and re-layouts  13.3 us (5%)
    all_to_all x5, waiting for transfers between devices, swap(): return lax.all_to_all(x, 'sp', split_axis=0, concat_axis=0, tiled=True)  94.8 us
    all_to_all x1, blocking collectives, swap(): return lax.all_to_all(x, 'sp', split_axis=0, concat_axis=0, tiled=True)  31.5 us
    pallas_call x1, Pallas kernels, attend(): pl.pallas_call(attend_kernel, out_shape=jax.ShapeDtypeStruct((blocks, row...  29.8 us
    pallas_call x2, Pallas kernels, expert(): pl.pallas_call(expert_kernel, grid=(ff // tile,), out_shape=jax.ShapeDtyp...  26 us
    all_to_all x5, starting transfers between devices, swap(): return lax.all_to_all(x, 'sp', split_axis=0, concat_axis=0, tiled=True)  20.1 us
    unnamed x41, local copies, waits for them, and re-layouts  13.3 us
    pallas_call x1, Pallas kernels, project(): pl.pallas_call(project_kernel, out_shape=(flat, flat, jax.ShapeDtypeStruc...  6.25 us
  transfers between devices with their start and end apart: 6, of which 5 were waited for; matrix products, arithmetic and copies ran while one was open for 0% of the time, Pallas kernels for 25%

profile of v1, /device:TPU:0, one launch (start us, length us, event | category | flops | bytes accessed | tf_op | source)
XLA Modules:
  0.0 244.7 jit_solution(2008956278013803883)
XLA Ops:
  9.1 1.0 copy-done.6
  10.2 1.0 copy-done.7
  11.7 31.5 %all_to_all.30.x_ref = bf16[16,400,128]{2,1,0:T(8,128)(2,1)S(1)} all-to-all(bf16[16,400,128]{2,1,0:T(8,128)(2,1)S(1)} %pack.1), channel_id=1, replica_groups=mesh['sp'=16,'dp'=8] {'sp'}, dimensions={0} | all-to-all | bytes 3276800 | tf_op jit(solution)/shard_map/all_to_all | solution.py:323
  43.2 29.8 %attend.1 = bf16[16,128,128]{2,1,0:T(8,128)(2,1)} custom-call(bf16[16,400,128]{2,1,0:T(8,128)(2,1)S(1)} %all_to_all.30.x_ref), custom_call_target="tpu_custom_call" | custom-call | tf_op jit(solution)/shard_map/attend/pallas_call | solution.py:131
  73.0 3.6 %all-to-all-start.1 = ((bf16[16,128,128]{2,1,0:T(8,128)(2,1)}), bf16[16,128,128]{2,1,0:T(8,128)(2,1)S(1)}, u32[]{:S(2)}, u32[]{:S(2)}) async-start(bf16[16,128,128]{2,1,0:T(8,128)(2,1)} %attend.1), calls=%async_computation.1 | async-start | bytes 1048576 | tf_op jit(solution)/shard_map/all_to_all | solution.py:323
  79.6 7.6 %all-to-all-done.1.a_ref = bf16[16,128,128]{2,1,0:T(8,128)(2,1)S(1)} async-done(((bf16[16,128,128]{2,1,0:T(8,128)(2,1)}), bf16[16,128,128]{2,1,0:T(8,128)(2,1)S(1)}, u32[]{:S(2)}, u32[]{:S(2)}) %all-to-all-start.1) | async-done | bytes 524320 | tf_op jit(solution)/shard_map/all_to_all | solution.py:323
  87.2 6.2 %project.1 = (bf16[256,2048]{1,0:T(8,128)(2,1)S(1)}, bf16[256,2048]{1,0:T(8,128)(2,1)S(1)}, bf16[512,2048]{1,0:T(8,128)(2,1)}) custom-call(bf16[16,128,128]{2,1,0:T(8,128)(2,1)S(1)} %all-to-all-done.1.a_ref, bf16[1024,2048]{1,0:T(8,128)(2,1)} %all-gather.2.cloned.1.call-done.w_ref, bf16[256,2048]{1,0:T(8,128)(2,1)S(1)} %bitcast.23, f32[1,2048]{1,0:T(1,128)S(1)} %bitcast.30, ...), custom_call_target="tpu_custom_call" | custom-call | tf_op jit(solution)/shard_map/project/pallas_call | solution.py:220
  94.5 4.4 %all-to-all-start.4 = ((bf16[16,32,2048]{2,1,0:T(8,128)(2,1)}), bf16[16,32,2048]{2,1,0:T(8,128)(2,1)}, u32[]{:S(2)}, u32[]{:S(2)}) async-start(bf16[16,32,2048]{2,1,0:T(8,128)(2,1)} %bitcast.16), calls=%async_computation.4 | async-start | bytes 4194304 | tf_op jit(solution)/shard_map/all_to_all | solution.py:323
  98.9 2.1 select_rows.1
  101.0 26.6 %all-to-all-done.4 = bf16[16,32,2048]{2,1,0:T(8,128)(2,1)} async-done(((bf16[16,32,2048]{2,1,0:T(8,128)(2,1)}), bf16[16,32,2048]{2,1,0:T(8,128)(2,1)}, u32[]{:S(2)}, u32[]{:S(2)}) %all-to-all-start.4) | async-done | bytes 2097184 | tf_op jit(solution)/shard_map/all_to_all | solution.py:323
  127.6 3.9 %all-to-all-start.2 = ((bf16[16,32,2048]{2,1,0:T(8,128)(2,1)}), bf16[16,32,2048]{2,1,0:T(8,128)(2,1)S(1)}, u32[]{:S(2)}, u32[]{:S(2)}) async-start(bf16[16,32,2048]{2,1,0:T(8,128)(2,1)} %bitcast.9), calls=%async_computation.2 | async-start | bytes 4194304 | tf_op jit(solution)/shard_map/all_to_all | solution.py:323
  131.5 13.0 %expert.3 = bf16[512,2048]{1,0:T(8,128)(2,1)} custom-call(bf16[512,2048]{1,0:T(8,128)(2,1)} %bitcast.17.x_ref, bf16[2048,1024]{1,0:T(8,128)(2,1)} %bitcast.36, bf16[2048,1024]{1,0:T(8,128)(2,1)} %bitcast.38, bf16[1024,2048]{1,0:T(8,128)(2,1)} %bitcast.40), custom_call_target="tpu_custom_call" | custom-call | flops 6442450944 | bytes 16000000 | tf_op jit(solution)/shard_map/expert/pallas_call | solution.py:269
  144.5 17.0 %all-to-all-done.2 = bf16[16,32,2048]{2,1,0:T(8,128)(2,1)S(1)} async-done(((bf16[16,32,2048]{2,1,0:T(8,128)(2,1)}), bf16[16,32,2048]{2,1,0:T(8,128)(2,1)S(1)}, u32[]{:S(2)}, u32[]{:S(2)}) %all-to-all-start.2) | async-done | bytes 2097184 | tf_op jit(solution)/shard_map/all_to_all | solution.py:323
  161.5 1.4 copy-done.16
  162.9 3.7 %all-to-all-start.5 = ((bf16[16,32,2048]{2,1,0:T(8,128)(2,1)}), bf16[16,32,2048]{2,1,0:T(8,128)(2,1)S(1)}, u32[]{:S(2)}, u32[]{:S(2)}) async-start(bf16[16,32,2048]{2,1,0:T(8,128)(2,1)} %bitcast.35), calls=%async_computation.5 | async-start | bytes 4194304 | tf_op jit(solution)/shard_map/all_to_all | solution.py:323
  166.6 13.0 %expert.2 = bf16[512,2048]{1,0:T(8,128)(2,1)} custom-call(bf16[512,2048]{1,0:T(8,128)(2,1)} %bitcast.33, bf16[2048,1024]{1,0:T(8,128)(2,1)} %bitcast.37, bf16[2048,1024]{1,0:T(8,128)(2,1)} %bitcast.39, bf16[1024,2048]{1,0:T(8,128)(2,1)} %bitcast.41), custom_call_target="tpu_custom_call" | custom-call | flops 6442450944 | bytes 16000000 | tf_op jit(solution)/shard_map/expert/pallas_call | solution.py:269
  179.6 17.7 %all-to-all-done.5 = bf16[16,32,2048]{2,1,0:T(8,128)(2,1)S(1)} async-done(((bf16[16,32,2048]{2,1,0:T(8,128)(2,1)}), bf16[16,32,2048]{2,1,0:T(8,128)(2,1)S(1)}, u32[]{:S(2)}, u32[]{:S(2)}) %all-to-all-start.5) | async-done | bytes 2097184 | tf_op jit(solution)/shard_map/all_to_all | solution.py:323
  197.3 4.4 %all-to-all-start.3 = ((bf16[16,32,2048]{2,1,0:T(8,128)(2,1)}), bf16[16,32,2048]{2,1,0:T(8,128)(2,1)}, u32[]{:S(2)}, u32[]{:S(2)}) async-start(bf16[16,32,2048]{2,1,0:T(8,128)(2,1)} %bitcast.34), calls=%async_computation.3 | async-start | bytes 4194304 | tf_op jit(solution)/shard_map/all_to_all | solution.py:323
  202.8 1.2 gather_sum.1.first_ref
  204.1 1.4 copy-done
  205.4 25.9 %all-to-all-done.3 = bf16[16,32,2048]{2,1,0:T(8,128)(2,1)} async-done(((bf16[16,32,2048]{2,1,0:T(8,128)(2,1)}), bf16[16,32,2048]{2,1,0:T(8,128)(2,1)}, u32[]{:S(2)}, u32[]{:S(2)}) %all-to-all-start.3) | async-done | bytes 2097184 | tf_op jit(solution)/shard_map/all_to_all | solution.py:323
  231.4 1.6 copy-done.1
  233.0 1.0 copy-done.11
  234.0 3.9 %finish.1 = bf16[256,2048]{1,0:T(8,128)(2,1)} custom-call(bf16[512,512]{1,0:T(8,128)(2,1)S(1)} %copy-done.11, bf16[512,2048]{1,0:T(8,128)(2,1)} %bitcast.15.x_ref, f32[256,2048]{1,0:T(8,128)S(1)} %copy-done.1, bf16[256,2048]{1,0:T(8,128)(2,1)S(1)} %copy-done.4, f32[1,2048]{1,0:T(1,128)S(1)} %bitcast.32), custom_call_target="tpu_custom_call" | custom-call | tf_op jit(solution)/shard_map/finish/pallas_call | solution.py:312
  (40 shorter events, 8.0 us)
Async XLA Ops:
  6.5 80.7 %all-gather.2.cloned.1.call-start = ((), (), s32[]{:S(2)}) async-start(), calls=%async_computation.6 | async-start | bytes 4718592 | tf_op jit(solution)/shard_map/all_gather | solution.py:345
  8.1 1.0 copy-start.5
  9.1 1.0 copy-start.6
  10.2 1.0 copy-start.7
  43.2 33.4 %copy-start.17 = (s32[1,256,2]{1,2,0:T(2,128)S(1)}, s32[1,256,2]{1,2,0:T(2,128)}, u32[]{:S(2)}) copy-start(s32[1,256,2]{1,2,0:T(2,128)} %param.24) | copy-start | bytes 6148
  43.2 33.6 %copy-start.18 = (f32[1,256,2]{1,2,0:T(2,128)S(1)}, f32[1,256,2]{1,2,0:T(2,128)}, u32[]{:S(2)}) copy-start(f32[1,256,2]{1,2,0:T(2,128)} %param.26) | copy-start | bytes 6148
  43.2 33.7 %copy-start.15 = (f32[1,256]{1,0:T(1,128)S(1)}, f32[1,256]{1,0:T(1,128)}, u32[]{:S(2)}) copy-start(f32[1,256]{1,0:T(1,128)} %gs_ref.1) | copy-start | bytes 3076
  43.2 44.0 %copy-start.2 = (bf16[1,256,2048]{2,1,0:T(8,128)(2,1)S(1)}, bf16[1,256,2048]{2,1,0:T(8,128)(2,1)}, u32[]{:S(2)}) copy-start(bf16[1,256,2048]{2,1,0:T(8,128)(2,1)} %param.15) | copy-start | bytes 3145732
  43.2 44.0 %copy-start.12 = (f32[2048]{0:T(1024)S(1)}, f32[2048]{0:T(1024)}, u32[]{:S(2)}) copy-start(f32[2048]{0:T(1024)} %param.21) | copy-start | bytes 24580
  43.2 44.0 %copy-start.13 = (f32[2048]{0:T(1024)S(1)}, f32[2048]{0:T(1024)}, u32[]{:S(2)}) copy-start(f32[2048]{0:T(1024)} %param.22) | copy-start | bytes 24580
  73.0 14.2 %all-to-all-start.1 = ((bf16[16,128,128]{2,1,0:T(8,128)(2,1)}), bf16[16,128,128]{2,1,0:T(8,128)(2,1)S(1)}, u32[]{:S(2)}, u32[]{:S(2)}) async-start(bf16[16,128,128]{2,1,0:T(8,128)(2,1)} %attend.1), calls=%async_computation.1 | async-start | bytes 1048576 | tf_op jit(solution)/shard_map/all_to_all | solution.py:323
  78.7 0.8 copy-start.10
  93.5 1.0 copy-start.3
  94.5 33.1 %all-to-all-start.4 = ((bf16[16,32,2048]{2,1,0:T(8,128)(2,1)}), bf16[16,32,2048]{2,1,0:T(8,128)(2,1)}, u32[]{:S(2)}, u32[]{:S(2)}) async-start(bf16[16,32,2048]{2,1,0:T(8,128)(2,1)} %bitcast.16), calls=%async_computation.4 | async-start | bytes 4194304 | tf_op jit(solution)/shard_map/all_to_all | solution.py:323
  127.6 33.9 %all-to-all-start.2 = ((bf16[16,32,2048]{2,1,0:T(8,128)(2,1)}), bf16[16,32,2048]{2,1,0:T(8,128)(2,1)S(1)}, u32[]{:S(2)}, u32[]{:S(2)}) async-start(bf16[16,32,2048]{2,1,0:T(8,128)(2,1)} %bitcast.9), calls=%async_computation.2 | async-start | bytes 4194304 | tf_op jit(solution)/shard_map/all_to_all | solution.py:323
  161.5 1.4 copy-start.16
  162.9 34.4 %all-to-all-start.5 = ((bf16[16,32,2048]{2,1,0:T(8,128)(2,1)}), bf16[16,32,2048]{2,1,0:T(8,128)(2,1)S(1)}, u32[]{:S(2)}, u32[]{:S(2)}) async-start(bf16[16,32,2048]{2,1,0:T(8,128)(2,1)} %bitcast.35), calls=%async_computation.5 | async-start | bytes 4194304 | tf_op jit(solution)/shard_map/all_to_all | solution.py:323
  197.3 34.1 %all-to-all-start.3 = ((bf16[16,32,2048]{2,1,0:T(8,128)(2,1)}), bf16[16,32,2048]{2,1,0:T(8,128)(2,1)}, u32[]{:S(2)}, u32[]{:S(2)}) async-start(bf16[16,32,2048]{2,1,0:T(8,128)(2,1)} %bitcast.34), calls=%async_computation.3 | async-start | bytes 4194304 | tf_op jit(solution)/shard_map/all_to_all | solution.py:323
  201.8 1.0 copy-start.9
  202.8 28.6 %copy-start.4 = (bf16[256,2048]{1,0:T(8,128)(2,1)S(1)}, bf16[256,2048]{1,0:T(8,128)(2,1)}, u32[]{:S(2)}) copy-start(bf16[256,2048]{1,0:T(8,128)(2,1)} %copy-done.3) | copy-start | bytes 3145732
  202.8 28.6 %copy-start.14 = (f32[2048]{0:T(1024)S(1)}, f32[2048]{0:T(1024)}, u32[]{:S(2)}) copy-start(f32[2048]{0:T(1024)} %param.23) | copy-start | bytes 24580
  204.0 1.4 copy-start
  231.4 1.6 copy-start.1
  233.0 1.0 copy-start.11
  (1 other events, 0.8 us)
Sparse Core Ops, SparseCore 0:
  9.0 37.9 all-gather.1
